TPU v7x, 32 devices: a whole 2x2x4 slice. The times are simulated.
32 devices in a mesh: kv: 8 (over y, x, core), tp: 4 (over z).
Axes of the slice: x: 2, y: 2, z: 4, core: 2. Of those that a mesh axis runs over, the one named last changes fastest.
Arguments:
- tokens: bfloat16 [64, 4, 4096], P(None, None, ('kv', 'tp')), may hold values from -36 to 36
- lengths: int32 [64], replicated, may hold values from 1 to 4, 112 in all
- state: float32 [64, 128, 4096], P('kv', None, 'tp'), may hold values from -0.6 to 0.6
- attn_gain: float32 [4096], P('kv'), may hold values from 0.1 to 1.9
- w_query: bfloat16 [4096, 4096], P('kv', 'tp'), may hold values from -0.09375 to 0.09375
- w_key: bfloat16 [4096, 4096], P('kv', 'tp'), may hold values from -0.09375 to 0.09375
- w_value: bfloat16 [4096, 4096], P('kv', 'tp'), may hold values from -0.09375 to 0.09375
- w_beta: bfloat16 [4096, 32], replicated, may hold values from -0.09375 to 0.09375
- w_alpha: bfloat16 [4096, 32], replicated, may hold values from -0.09375 to 0.09375
- decay_rate: float32 [32], replicated, may hold values from 0.05 to 3
- decay_bias: float32 [32], replicated, may hold values from -3 to 3
- out_gain: float32 [128], replicated, may hold values from 0.1 to 1.9
- w_out: bfloat16 [4096, 4096], P('tp', 'kv'), may hold values from -0.09375 to 0.09375
- mix_gain: float32 [4096], P('kv'), may hold values from 0.1 to 1.9
- w_gate: bfloat16 [4096, 11008], P('kv', 'tp'), may hold values from -0.09375 to 0.09375
- w_up: bfloat16 [4096, 11008], P('kv', 'tp'), may hold values from -0.09375 to 0.09375
- w_down: bfloat16 [11008, 4096], P('tp', 'kv'), may hold values from -0.0546875 to 0.0546875
Outputs:
- mixed: bfloat16 [64, 4, 4096], P(None, None, ('kv', 'tp'))
- new_state: float32 [64, 128, 4096], P('kv', None, 'tp')
Inputs may be any that keep to these rules, and one draw needn't show every extreme that they name: Each sequence has 1 to 4 live tokens, the first ones of its block, and the lengths sum to 112.
All inputs are finite; a program needn't handle non-finite values.
Results may differ from a plain program's by a relative error of at most 0.015.
Values may be sent and summed in bfloat16 or wider, within the bound.
A program may use at most 64 MiB of HBM per device.

v0:
```python
import jax
import jax.numpy as jnp
from jax import lax
from jax.sharding import PartitionSpec as P

D = 4096
HEAD_DIM = 128
EPSILON = 1e-06


def unit_rows(vectors):
    return vectors * lax.rsqrt(jnp.sum(vectors * vectors, axis=-1, keepdims=True) + EPSILON)


def delta_block(queries, unit_keys, values_split, beta, log_decay, carried):
    highest = lax.Precision.HIGHEST
    seq_count, span_len, heads_here = beta.shape
    cumulative = jnp.cumsum(log_decay, axis=1)
    position = jnp.arange(span_len)
    inclusive = (position[:, None] >= position[None, :])[None, :, :, None]
    strict = (position[:, None] > position[None, :])[None, :, :, None]
    gap_matrix = cumulative[:, :, None, :] - cumulative[:, None, :, :]
    decay_matrix = jnp.where(inclusive, jnp.exp(jnp.where(inclusive, gap_matrix, 0.0)), 0.0)
    key_dots = jnp.einsum("nihd,njhd->nijh", unit_keys, unit_keys, precision=highest)
    query_dots = jnp.einsum("nihd,njhd->nijh", queries, unit_keys, precision=highest) * decay_matrix
    lower_part = jnp.where(strict, key_dots * decay_matrix * beta[:, :, None, :], 0.0)
    identity = jnp.eye(span_len, dtype=jnp.float32)
    inverse_rows = []
    for step in range(span_len):
        row_now = jnp.broadcast_to(identity[step][None, :, None], (seq_count, span_len, heads_here))
        for prior in range(step):
            row_now = row_now - lower_part[:, step, prior, :][:, None, :] * inverse_rows[prior]
        inverse_rows.append(row_now)
    inverse = jnp.stack(inverse_rows, axis=1)
    beta_value = beta[..., None] * values_split
    beta_key = (beta * jnp.exp(cumulative))[..., None] * unit_keys
    base_update = jnp.einsum("nich,nche->nihe", inverse, beta_value, precision=highest)
    key_weights = jnp.einsum("nich,nchd->nihd", inverse, beta_key, precision=highest)
    corrected = base_update - jnp.einsum("nihd,ndhe->nihe", key_weights, carried, precision=highest)
    decayed_queries = queries * jnp.exp(cumulative)[..., None]
    attended = jnp.einsum("nihd,ndhe->nihe", decayed_queries, carried, precision=highest)
    attended = attended + jnp.einsum("nijh,njhe->nihe", query_dots, corrected, precision=highest)
    block_total = cumulative[:, -1, :]
    key_tail = unit_keys * jnp.exp(block_total[:, None, :] - cumulative)[..., None]
    updated = carried * jnp.exp(block_total)[:, None, :, None]
    updated = updated + jnp.einsum("nihd,nihe->ndhe", key_tail, corrected, precision=highest)
    return (attended, updated)


def body(
    tokens,
    lengths,
    state,
    attn_gain,
    w_query,
    w_key,
    w_value,
    w_beta,
    w_alpha,
    decay_rate,
    decay_bias,
    out_gain,
    w_out,
    mix_gain,
    w_gate,
    w_up,
    w_down,
):
    kv_index = lax.axis_index("kv")
    tp_index = lax.axis_index("tp")
    kv_count = lax.axis_size("kv")
    batch_all, span_len, own_cols = tokens.shape
    row_count = batch_all * span_len
    seq_count = state.shape[0]
    local_rows = seq_count * span_len
    head_size = state.shape[1]
    heads_here = state.shape[2] // head_size
    block_width = attn_gain.shape[0]
    flat_rows = tokens.reshape(row_count, own_cols)
    live_all = (jnp.arange(span_len, dtype=jnp.int32)[None, :] < lengths[:, None]).reshape(
        row_count, 1
    )
    gathered = lax.all_gather(flat_rows, "tp", axis=1, tiled=True).astype(jnp.float32)
    squares_in = jnp.sum(gathered * gathered, axis=1)
    normed_in = (gathered * attn_gain).astype(jnp.bfloat16)
    beta_rows = lax.dynamic_slice_in_dim(w_beta, kv_index * block_width, block_width, 0)
    alpha_rows = lax.dynamic_slice_in_dim(w_alpha, kv_index * block_width, block_width, 0)
    query_part = jnp.dot(normed_in, w_query, preferred_element_type=jnp.float32)
    key_part = jnp.dot(normed_in, w_key, preferred_element_type=jnp.float32)
    value_part = jnp.dot(normed_in, w_value, preferred_element_type=jnp.float32)
    beta_part = jnp.dot(normed_in, beta_rows, preferred_element_type=jnp.float32)
    alpha_part = jnp.dot(normed_in, alpha_rows, preferred_element_type=jnp.float32)
    squares_all = lax.psum(squares_in, "kv")
    squares_own = lax.dynamic_slice_in_dim(squares_all, kv_index * local_rows, local_rows, 0)
    query_sum, key_sum, value_sum, beta_sum, alpha_sum = (
        lax.psum_scatter(
            query_part.astype(jnp.bfloat16), "kv", scatter_dimension=0, tiled=True
        ).astype(jnp.float32),
        lax.psum_scatter(
            key_part.astype(jnp.bfloat16), "kv", scatter_dimension=0, tiled=True
        ).astype(jnp.float32),
        lax.psum_scatter(
            value_part.astype(jnp.bfloat16), "kv", scatter_dimension=0, tiled=True
        ).astype(jnp.float32),
        lax.psum_scatter(
            beta_part.astype(jnp.bfloat16), "kv", scatter_dimension=0, tiled=True
        ).astype(jnp.float32),
        lax.psum_scatter(
            alpha_part.astype(jnp.bfloat16), "kv", scatter_dimension=0, tiled=True
        ).astype(jnp.float32),
    )
    row_scale = lax.rsqrt(squares_own / D + EPSILON)[:, None]
    head_start = tp_index * heads_here
    lengths_own = lax.dynamic_slice_in_dim(lengths, kv_index * seq_count, seq_count, 0)
    live_own = (jnp.arange(span_len, dtype=jnp.int32)[None, :] < lengths_own[:, None])[..., None]
    beta_heads = lax.dynamic_slice_in_dim(beta_sum, head_start, heads_here, 1) * row_scale
    alpha_heads = lax.dynamic_slice_in_dim(alpha_sum, head_start, heads_here, 1) * row_scale
    rate_here = lax.dynamic_slice_in_dim(decay_rate, head_start, heads_here, 0)
    bias_here = lax.dynamic_slice_in_dim(decay_bias, head_start, heads_here, 0)
    beta = jnp.where(
        live_own, jax.nn.sigmoid(beta_heads).reshape(seq_count, span_len, heads_here), 0.0
    )
    log_decay = -rate_here * jax.nn.softplus(alpha_heads + bias_here)
    log_decay = jnp.where(live_own, log_decay.reshape(seq_count, span_len, heads_here), 0.0)
    split_shape = (seq_count, span_len, heads_here, head_size)
    queries = unit_rows((query_sum * row_scale).reshape(split_shape)) * HEAD_DIM ** (-0.5)
    unit_keys = unit_rows((key_sum * row_scale).reshape(split_shape))
    values_split = (value_sum * row_scale).reshape(split_shape)
    carried = state.reshape(seq_count, head_size, heads_here, head_size)
    attended, updated = delta_block(queries, unit_keys, values_split, beta, log_decay, carried)
    head_out = (
        attended
        * lax.rsqrt(jnp.mean(attended * attended, axis=-1, keepdims=True) + EPSILON)
        * out_gain
    )
    head_out = head_out.astype(jnp.bfloat16).reshape(local_rows, heads_here * head_size)
    pack_rows = min((batch_all * 7 // 4 + kv_count - 1) // kv_count * kv_count, row_count)
    live_flat = live_all.reshape(row_count).astype(jnp.int32)
    slot_index = jnp.cumsum(live_flat) - 1
    picker = (
        (slot_index[None, :] == jnp.arange(pack_rows, dtype=jnp.int32)[:, None])
        & (live_flat[None, :] > 0)
    ).astype(jnp.bfloat16)
    heads_every = lax.all_gather(head_out, "kv", axis=0, tiled=True)
    packed_heads = jnp.dot(picker, heads_every, preferred_element_type=jnp.float32).astype(
        jnp.bfloat16
    )
    attn_part = jnp.dot(packed_heads, w_out, preferred_element_type=jnp.float32)
    base_rows = jnp.dot(picker, flat_rows, preferred_element_type=jnp.float32)
    attn_own = lax.psum_scatter(
        attn_part.astype(jnp.bfloat16), "tp", scatter_dimension=1, tiled=True
    ).astype(jnp.float32)
    middle = (base_rows + attn_own).astype(jnp.bfloat16)
    middle_rows = lax.all_gather(middle, "tp", axis=1, tiled=True).astype(jnp.float32)
    squares_mid = jnp.sum(middle_rows * middle_rows, axis=1)
    normed_mid = (middle_rows * mix_gain).astype(jnp.bfloat16)
    gate_part = jnp.dot(normed_mid, w_gate, preferred_element_type=jnp.float32)
    up_part = jnp.dot(normed_mid, w_up, preferred_element_type=jnp.float32)
    squares_total = lax.psum(squares_mid, "kv")
    gate_sum, up_sum = (
        lax.psum(gate_part.astype(jnp.bfloat16), "kv").astype(jnp.float32),
        lax.psum(up_part.astype(jnp.bfloat16), "kv").astype(jnp.float32),
    )
    mid_scale = lax.rsqrt(squares_total / D + EPSILON)[:, None]
    hidden = (jax.nn.silu(gate_sum * mid_scale) * (up_sum * mid_scale)).astype(jnp.bfloat16)
    down_part = jnp.dot(hidden, w_down, preferred_element_type=jnp.float32)
    down_own = lax.psum_scatter(
        down_part.astype(jnp.bfloat16), "tp", scatter_dimension=1, tiled=True
    ).astype(jnp.float32)
    result_rows = middle.astype(jnp.float32) + down_own
    result_rows = jnp.dot(
        picker.astype(jnp.float32).T,
        result_rows,
        precision=lax.Precision.HIGHEST,
        preferred_element_type=jnp.float32,
    )
    mixed = (
        jnp.where(live_all, result_rows, 0.0)
        .astype(jnp.bfloat16)
        .reshape(batch_all, span_len, own_cols)
    )
    return (mixed, updated.reshape(seq_count, head_size, heads_here * head_size))


def solution(mesh):
    return jax.shard_map(
        body,
        mesh=mesh,
        in_specs=(
            P(None, None, ("kv", "tp")),
            P(),
            P("kv", None, "tp"),
            P("kv"),
            P("kv", "tp"),
            P("kv", "tp"),
            P("kv", "tp"),
            P(),
            P(),
            P(),
            P(),
            P(),
            P("tp", "kv"),
            P("kv"),
            P("kv", "tp"),
            P("kv", "tp"),
            P("tp", "kv"),
        ),
        out_specs=(P(None, None, ("kv", "tp")), P("kv", None, "tp")),
        check_vma=False,
    )
```

profile of v0, /device:TPU:0, one launch (start us, length us, event | category | flops | bytes accessed | tf_op | source)
XLA Modules:
  0.0 369.6 jit_solution(18087534690063010372)
XLA Ops:
  7.2 14.8 %all_gather.9 = bf16[256,512]{1,0:T(8,128)(2,1)S(1)} all-gather(bf16[256,128]{1,0:T(8,128)(2,1)} %bitcast.99), channel_id=1, replica_groups=mesh['kv'=8,'tp'=4] {'tp'}, dimensions={1}, use_global_device_ids=true | all-gather | bytes 327680 | tf_op jit(solution)/shard_map/all_gather | solution.py:83
  22.1 1.6 convolution_convert_fusion.7
  23.8 1.6 convolution_convert_fusion.8
  25.5 2.5 convolution_convert_fusion.4
  28.0 2.5 convolution_convert_fusion.3
  30.6 2.5 convolution_convert_fusion.2
  33.1 0.1 fusion.13
  33.4 0.1 lt.80
  33.5 0.1 lt.76
  33.6 12.2 %psum.28 = f32[256]{0:T(256)S(1)} all-reduce(f32[256]{0:T(256)S(1)} %fusion.13), channel_id=1, replica_groups=mesh['kv'=8,'tp'=4] {'kv'}, use_global_device_ids=true, to_apply=%region_4.0 | all-reduce | flops 256 | bytes 2048 | tf_op jit(solution)/shard_map/psum | solution.py:93
  46.1 5.3 %copy.107 = f32[8,128,1024]{1,2,0:T(8,128)} copy(f32[8,128,1024]{2,1,0:T(8,128)} %param.19) | data formatting | bytes 8388608 | tf_op args[2]
  51.5 0.1 lt.82
  51.6 0.1 lt.78
  51.7 0.3 reduce-window.9
  52.1 0.1 slice_reduce_fusion.6
  52.2 0.7 add_bitcast_fusion
  52.9 0.5 convert_compare_fusion
  53.4 0.1 add_rsqrt_fusion.2
  53.5 4.4 %reduce-scatter.16.cloned.1.call-done = bf16[32,32]{1,0:T(8,128)(2,1)} async-done(((bf16[256,32]{1,0:T(8,128)(2,1)}), bf16[32,32]{1,0:T(8,128)(2,1)}) %reduce-scatter.16.cloned.1.call-update) | async-done | bytes 2064 | tf_op jit(solution)/shard_map/reduce_scatter | solution.py:105
  57.9 36.5 %reduce-scatter.14.cloned.1.call-done = bf16[32,32]{1,0:T(8,128)(2,1)} async-done(((bf16[256,32]{1,0:T(8,128)(2,1)}), bf16[32,32]{1,0:T(8,128)(2,1)}) %reduce-scatter.14.cloned.1.call-update) | async-done | bytes 2064 | tf_op jit(solution)/shard_map/reduce_scatter | solution.py:108
  94.4 0.8 add_divide_fusion
  95.3 0.1 copy.117
  95.4 0.1 exponential_multiply_fusion
  95.5 0.1 copy.111
  95.6 36.0 %reduce-scatter.12.cloned.1.call-done = bf16[32,1024]{1,0:T(8,128)(2,1)} async-done(((bf16[256,1024]{1,0:T(8,128)(2,1)}), bf16[32,1024]{1,0:T(8,128)(2,1)}) %reduce-scatter.12.cloned.1.call-update) | async-done | bytes 65552 | tf_op jit(solution)/shard_map/reduce_scatter | solution.py:96
  131.6 37.1 %reduce-scatter.18.cloned.1.call-done = bf16[32,1024]{1,0:T(8,128)(2,1)} async-done(((bf16[256,1024]{1,0:T(8,128)(2,1)}), bf16[32,1024]{1,0:T(8,128)(2,1)}) %reduce-scatter.18.cloned.1.call-update) | async-done | bytes 65552 | tf_op jit(solution)/shard_map/reduce_scatter | solution.py:102
  168.7 37.1 %reduce-scatter.20.cloned.1.call-done = bf16[32,1024]{1,0:T(8,128)(2,1)} async-done(((bf16[256,1024]{1,0:T(8,128)(2,1)}), bf16[32,1024]{1,0:T(8,128)(2,1)}) %reduce-scatter.20.cloned.1.call-update) | async-done | bytes 65552 | tf_op jit(solution)/shard_map/reduce_scatter | solution.py:99
  205.8 1.0 multiply_bitcast_fusion.2
  206.8 0.1 multiply_reduce_fusion.2
  207.0 0.1 multiply_reduce_fusion.1
  207.2 0.9 multiply_multiply_fusion.1
  208.1 0.6 fusion.6
  208.6 1.1 slice_reduce_fusion.4
  209.7 0.1 multiply_subtract_fusion.1
  209.9 0.3 copy.120
  210.2 0.1 broadcast_multiply_fusion.1
  210.3 1.4 convolution_bitcast_fusion.5
  211.7 0.6 convolution_bitcast_fusion.4
  212.2 1.6 fusion.7
  213.9 8.6 %fusion.2 = f32[8,4,8,128]{3,1,2,0:T(4,128)S(1)} fusion(f32[8,4,8,128]{3,1,2,0:T(4,128)S(1)} %convolution_bitcast_fusion.5, f32[8,4,8,128]{3,1,2,0:T(4,128)S(1)} %convolution_bitcast_fusion.4, f32[8,128,8,128]{1,3,2,0:T(8,128)} %bitcast.86), kind=kOutput, calls=%fused_computation.12 | convolution fusion | flops 50364416 | bytes 4587520 | tf_op jit(solution)/shard_map/nihd,ndhe->nihe/dot_general | solution.py:39
  222.5 0.7 convolution_bitcast_fusion.2
  223.2 6.7 %multiply_reduce_fusion = (f32[8,4,8]{1,2,0:T(8,128)S(1)}, f32[8,4,8,128]{3,1,2,0:T(4,128)S(1)}) fusion(f32[8,4,8,128]{3,1,2,0:T(4,128)S(1)} %convolution_bitcast_fusion.2, f32[8,128,8,128]{1,3,2,0:T(8,128)S(1)} %bitcast.88, f32[8,4,8,128]{3,2,1,0:T(8,128)S(1)} %get-tuple-element.24), kind=kOutput, calls=%fused_computation.46 | convolution fusion | flops 50429696 | bytes 4588544 | tf_op jit(solution)/shard_map/nihd,ndhe->nihe/dot_general | solution.py:41
  229.9 0.1 copy.128
  230.0 0.1 copy.129
  230.1 0.1 multiply_convert_fusion.2
  230.3 9.8 %all_gather.10 = bf16[256,1024]{1,0:T(8,128)(2,1)S(1)} all-gather(bf16[32,1024]{1,0:T(8,128)(2,1)S(1)} %bitcast.96), channel_id=1, replica_groups=mesh['kv'=8,'tp'=4] {'kv'}, dimensions={0}, use_global_device_ids=true | all-gather | bytes 589824 | tf_op jit(solution)/shard_map/all_gather | solution.py:144
  240.1 2.3 fusion.1
  242.4 1.7 copy.137
  244.2 19.5 %reduce-scatter.22.cloned.1.call-done = bf16[128,112]{1,0:T(8,128)(2,1)} async-done(((bf16[512,112]{1,0:T(8,128)(2,1)}), bf16[128,112]{1,0:T(8,128)(2,1)}) %reduce-scatter.22.cloned.1.call-update) | async-done | bytes 28688
  263.7 0.9 copy.138
  264.6 1.0 fusion.9
  265.5 12.2 %all_gather.11 = bf16[112,512]{1,0:T(8,128)(2,1)S(1)} all-gather(bf16[112,128]{1,0:T(8,128)(2,1)S(1)} %fusion.9), channel_id=1, replica_groups=mesh['kv'=8,'tp'=4] {'tp'}, dimensions={1}, use_global_device_ids=true | all-gather | bytes 143360 | tf_op jit(solution)/shard_map/all_gather | solution.py:154
  277.7 2.6 convolution_convert_fusion
  280.3 1.8 convolution_convert_fusion.1
  282.2 0.1 fusion.15
  282.3 12.1 %psum.30 = f32[112]{0:T(128)S(1)} all-reduce(f32[112]{0:T(128)S(1)} %fusion.15), channel_id=1, replica_groups=mesh['kv'=8,'tp'=4] {'kv'}, use_global_device_ids=true, to_apply=%region_16.17 | all-reduce | flops 112 | bytes 896 | tf_op jit(solution)/shard_map/psum | solution.py:159
  294.5 44.0 %all-reduce.3.cloned.1.call-done = (bf16[112,2752]{1,0:T(8,128)(2,1)}, bf16[112,2752]{1,0:T(8,128)(2,1)}) async-done(((bf16[112,2752]{1,0:T(8,128)(2,1)}, bf16[112,2752]{1,0:T(8,128)(2,1)}), (bf16[112,2752]{1,0:T(8,128)(2,1)}, bf16[112,2752]{1,0:T(8,128)(2,1)})) %all-reduce.3.cloned.1.call-update) | async-done | bytes 1232912 | tf_op jit(solution)/shard_map/psum | solution.py:162
  338.5 2.9 convolution_convert_fusion.6
  341.4 0.7 copy.139
  342.2 10.2 %bitcast_add_fusion = f32[8,128,8,128]{1,3,2,0:T(8,128)} fusion(f32[8,128,8,128]{1,3,2,0:T(8,128)} %bitcast.87, f32[8,4,8,128]{3,1,2,0:T(4,128)S(1)} %fusion.2, f32[8,8]{1,0:T(8,128)S(1)} %fusion.59, f32[8,4,8,128]{3,2,1,0:T(8,128)S(1)} %copy-done.3), kind=kOutput, calls=%fused_computation | convolution fusion | flops 52428800 | bytes 8651008 | tf_op jit(solution)/shard_map/nihd,nihe->ndhe/dot_general | solution.py:46
  352.4 5.4 %copy.133 = f32[8,128,1024]{2,1,0:T(8,128)} copy(f32[8,128,1024]{1,2,0:T(8,128)} %bitcast.89) | data formatting | bytes 8388608
  357.8 3.2 reduce-scatter.24.cloned.1.call-done
  360.9 0.9 copy.140
  361.8 0.9 fusion.8
  (80 shorter events, 1.4 us)
Async XLA Ops:
  7.2 270.6 %copy-start = (bf16[512,2752]{0,1:T(8,128)(2,1)S(1)}, bf16[512,2752]{0,1:T(8,128)(2,1)}, u32[]{:S(2)}) copy-start(bf16[512,2752]{0,1:T(8,128)(2,1)} %param.32) | copy-start | bytes 8454148
  7.2 20.8 %copy-start.6 = (f32[512]{0:T(512)S(1)}, f32[512]{0:T(512)}, u32[]{:S(2)}) copy-start(f32[512]{0:T(512)} %param.20) | copy-start | bytes 6148
  7.2 50.7 %reduce-scatter.16.cloned.1.call-start = ((), (), s32[]{:S(2)}) async-start(), calls=%async_computation.9 | async-start | bytes 73728 | tf_op jit(solution)/shard_map/reduce_scatter | solution.py:105
  23.7 70.7 %reduce-scatter.14.cloned.1.call-start = ((), (), s32[]{:S(2)}) async-start(), calls=%async_computation.8 | async-start | bytes 73728 | tf_op jit(solution)/shard_map/reduce_scatter | solution.py:108
  25.4 106.2 %reduce-scatter.12.cloned.1.call-start = ((), (), s32[]{:S(2)}) async-start(), calls=%async_computation.7 | async-start | bytes 589824 | tf_op jit(solution)/shard_map/reduce_scatter | solution.py:96
  27.9 5.4 %copy-start.11 = (s32[64]{0:T(128)S(1)}, s32[64]{0:T(128)}, u32[]{:S(2)}) copy-start(s32[64]{0:T(128)} %param.18) | copy-start | bytes 772
  27.9 17.9 %copy-start.14 = (f32[32]{0:T(128)S(1)}, f32[32]{0:T(128)}, u32[]{:S(2)}) copy-start(f32[32]{0:T(128)} %param.27) | copy-start | bytes 388
  27.9 18.0 %copy-start.15 = (f32[32]{0:T(128)S(1)}, f32[32]{0:T(128)}, u32[]{:S(2)}) copy-start(f32[32]{0:T(128)} %param.26) | copy-start | bytes 388
  28.0 140.8 %reduce-scatter.18.cloned.1.call-start = ((), (), s32[]{:S(2)}) async-start(), calls=%async_computation.10 | async-start | bytes 589824 | tf_op jit(solution)/shard_map/reduce_scatter | solution.py:102
  30.5 175.3 %reduce-scatter.20.cloned.1.call-start = ((), (), s32[]{:S(2)}) async-start(), calls=%async_computation.11 | async-start | bytes 589824 | tf_op jit(solution)/shard_map/reduce_scatter | solution.py:99
  33.1 230.6 %reduce-scatter.22.cloned.1.call-start = ((), (), s32[]{:S(2)}) async-start(), calls=%async_computation.12 | async-start | bytes 163840
  33.6 19.3 %copy-start.12 = (pred[256]{0:T(512)(128)(4,1)}, pred[256]{0:T(512)(128)(4,1)S(1)}, u32[]{:S(2)}) copy-start(pred[256]{0:T(512)(128)(4,1)S(1)} %lt.76) | copy-start | bytes 772
  95.6 114.2 %copy-start.5 = (f32[8,4,8]{1,2,0:T(8,128)}, f32[8,4,8]{1,2,0:T(8,128)S(1)}, u32[]{:S(2)}) copy-start(f32[8,4,8]{1,2,0:T(8,128)S(1)} %copy.111) | copy-start | bytes 3076
  212.2 10.9 %copy-start.1 = (f32[8,128,1024]{1,2,0:T(8,128)S(1)}, f32[8,128,1024]{1,2,0:T(8,128)}, u32[]{:S(2)}) copy-start(f32[8,128,1024]{1,2,0:T(8,128)} %copy.107) | copy-start | bytes 12582916
  222.5 7.7 %copy-start.9 = (f32[128]{0:T(128)S(1)}, f32[128]{0:T(128)}, u32[]{:S(2)}) copy-start(f32[128]{0:T(128)} %param.28) | copy-start | bytes 1540
  229.9 34.7 %copy-start.4 = (bf16[64,4,128]{2,1,0:T(4,128)(2,1)S(1)}, bf16[64,4,128]{2,1,0:T(4,128)(2,1)}, u32[]{:S(2)}) copy-start(bf16[64,4,128]{2,1,0:T(4,128)(2,1)} %param.17) | copy-start | bytes 196612
  242.4 37.9 %copy-start.7 = (f32[512]{0:T(512)S(1)}, f32[512]{0:T(512)}, u32[]{:S(2)}) copy-start(f32[512]{0:T(512)} %param.30) | copy-start | bytes 6148
  244.1 94.4 %all-reduce.3.cloned.1.call-start = ((), (), s32[]{:S(2)}) async-start(), calls=%async_computation.14 | async-start | bytes 2523136 | tf_op jit(solution)/shard_map/psum | solution.py:162
  264.6 15.7 %copy-start.2 = (bf16[512,2752]{0,1:T(8,128)(2,1)S(1)}, bf16[512,2752]{0,1:T(8,128)(2,1)}, u32[]{:S(2)}) copy-start(bf16[512,2752]{0,1:T(8,128)(2,1)} %param.31) | copy-start | bytes 8454148
  282.2 78.8 %reduce-scatter.24.cloned.1.call-start = ((), (), s32[]{:S(2)}) async-start(), calls=%async_computation.13 | async-start | bytes 163840
  338.5 3.7 copy-start.3
  352.4 9.4 %copy-start.8 = (s32[256]{0:T(256)S(1)}, s32[256]{0:T(256)}, u32[]{:S(2)}) copy-start(s32[256]{0:T(256)} %add_bitcast_fusion) | copy-start | bytes 3076
  352.4 9.4 %copy-start.10 = (pred[256]{0:T(512)(128)(4,1)S(1)}, pred[256]{0:T(512)(128)(4,1)}, u32[]{:S(2)}) copy-start(pred[256]{0:T(512)(128)(4,1)} %convert_compare_fusion) | copy-start | bytes 772
  352.4 9.4 %copy-start.13 = (pred[256]{0:T(512)(128)(4,1)S(1)}, pred[256]{0:T(512)(128)(4,1)}, u32[]{:S(2)}) copy-start(pred[256]{0:T(512)(128)(4,1)} %copy-done.12) | copy-start | bytes 772
Sparse Core Ops, SparseCore 0:
  23.8 34.0 reduce-scatter.15
  60.9 33.4 reduce-scatter.13
  97.5 34.1 reduce-scatter.11
  134.6 34.1 reduce-scatter.17
  171.6 34.1 reduce-scatter.19
  244.2 19.4 reduce-scatter.21
  282.3 56.1 all-reduce.2
  342.3 18.6 reduce-scatter.23
where the time goes:
time: 371 us; the launch traced here: 370 us
  waiting for transfers between devices  218 us (59%)
  blocking collectives  61.2 us (16%)
  matrix products  52.5 us (14%)
  local copies, waits for them, and re-layouts  17.7 us (5%)
  between operations  14.5 us (4%)
  other arithmetic  5.46 us (1%)
    psum x1, waiting for transfers between devices, body(): lax.psum(up_part.astype(jnp.bfloat16), 'kv').astype(jnp.float32)  44 us
    reduce_scatter x1, waiting for transfers between devices, body(): lax.psum_scatter(value_part.astype(jnp.bfloat16), 'kv', scatter_dimension...  37.1 us
    reduce_scatter x1, waiting for transfers between devices, body(): lax.psum_scatter(key_part.astype(jnp.bfloat16), 'kv', scatter_dimension=0...  37.1 us
    reduce_scatter x1, waiting for transfers between devices, body(): lax.psum_scatter(alpha_part.astype(jnp.bfloat16), 'kv', scatter_dimension...  36.5 us
    reduce_scatter x1, waiting for transfers between devices, body(): lax.psum_scatter(query_part.astype(jnp.bfloat16), 'kv', scatter_dimension...  36 us
    unnamed x10, waiting for transfers between devices  22.8 us
    unnamed x42, local copies, waits for them, and re-layouts  15 us
    all_gather x1, blocking collectives, body(): lax.all_gather(flat_rows, 'tp', axis=1, tiled=True).astype(jnp.float32)  14.8 us
  transfers between devices with their start and end apart: 8, of which 8 were waited for; matrix products, arithmetic and copies ran while one was open for 9% of the time, Pallas kernels for 0%

commit v1 on v0

--- a/solution.py
+++ b/solution.py
@@ -159,7 +159,7 @@
     squares_total = lax.psum(squares_mid, "kv")
     gate_sum, up_sum = (
         lax.psum(gate_part.astype(jnp.bfloat16), "kv").astype(jnp.float32),
-        lax.psum(up_part.astype(jnp.bfloat16), "kv").astype(jnp.float32),
+        jnp.sum(lax.all_gather(up_part.astype(jnp.bfloat16), "kv"), axis=0).astype(jnp.float32),
     )
     mid_scale = lax.rsqrt(squares_total / D + EPSILON)[:, None]
     hidden = (jax.nn.silu(gate_sum * mid_scale) * (up_sum * mid_scale)).astype(jnp.bfloat16)

time: 371 us -> 410 us (1.11)
  waiting for transfers between devices: 218 us -> 250 us
  other arithmetic: 5.46 us -> 10.2 us
    reduce_scatter x1, waiting for transfers between devices: 36.5 us -> 3.69 us  [body(): lax.psum_scatter(alpha_part.astype(jnp.bfloat16), 'kv', scatter_dimension...]
    reduce_scatter x1, waiting for transfers between devices: 4.39 us -> 37.1 us  [body(): lax.psum_scatter(beta_part.astype(jnp.bfloat16), 'kv', scatter_dimension=...]
    all_gather x0 -> x1, waiting for transfers between devices: none -> 22.3 us  [body(): lax.all_gather(up_part.astype(jnp.bfloat16), 'kv')]
    psum x1, waiting for transfers between devices: 44 us -> 54.2 us  [body(): lax.psum(gate_part.astype(jnp.bfloat16), 'kv').astype(jnp.float32)]
    reduce_sum x0 -> x1, other arithmetic: none -> 4.15 us  [body(): jnp.sum(lax.all_gather(up_part.astype(jnp.bfloat16), 'kv'), axis=0)]
    unnamed x10 -> x11, waiting for transfers between devices: 22.8 us -> 23.1 us
  transfers between devices with their start and end apart: 8 -> 9, of which waited for: 8 -> 9; matrix products, arithmetic and copies ran while one was open for 9% -> 11% of each run, Pallas kernels for 0% -> 0%
where the time goes in v1:
time: 410 us; the launch traced here: 409 us
  waiting for transfers between devices  250 us (61%)
  blocking collectives  61.6 us (15%)
  matrix products  54.3 us (13%)
  local copies, waits for them, and re-layouts  18.3 us (4%)
  between operations  14.2 us (3%)
  other arithmetic  10.2 us (2%)
    psum x1, waiting for transfers between devices, body(): lax.psum(gate_part.astype(jnp.bfloat16), 'kv').astype(jnp.float32)  54.2 us
    reduce_scatter x1, waiting for transfers between devices, body(): lax.psum_scatter(key_part.astype(jnp.bfloat16), 'kv', scatter_dimension=0...  37.1 us
    reduce_scatter x1, waiting for transfers between devices, body(): lax.psum_scatter(beta_part.astype(jnp.bfloat16), 'kv', scatter_dimension=...  37.1 us
    reduce_scatter x1, waiting for transfers between devices, body(): lax.psum_scatter(query_part.astype(jnp.bfloat16), 'kv', scatter_dimension...  37.1 us
    reduce_scatter x1, waiting for transfers between devices, body(): lax.psum_scatter(value_part.astype(jnp.bfloat16), 'kv', scatter_dimension...  35.4 us
    unnamed x11, waiting for transfers between devices  23.1 us
    all_gather x1, waiting for transfers between devices, body(): lax.all_gather(up_part.astype(jnp.bfloat16), 'kv')  22.3 us
    unnamed x42, local copies, waits for them, and re-layouts  14.9 us
  transfers between devices with their start and end apart: 9, of which 9 were waited for; matrix products, arithmetic and copies ran while one was open for 11% of the time, Pallas kernels for 0%

profile of v1, /device:TPU:0, one launch (start us, length us, event | category | flops | bytes accessed | tf_op | source)
XLA Modules:
  0.0 409.1 jit_solution(5718477485555910404)
XLA Ops:
  7.2 14.8 %all_gather.15 = bf16[256,512]{1,0:T(8,128)(2,1)S(1)} all-gather(bf16[256,128]{1,0:T(8,128)(2,1)} %bitcast.101), channel_id=1, replica_groups=mesh['kv'=8,'tp'=4] {'tp'}, dimensions={1}, use_global_device_ids=true | all-gather | bytes 327680 | tf_op jit(solution)/shard_map/all_gather | solution.py:83
  22.1 1.6 convolution_convert_fusion.8
  23.8 1.6 convolution_convert_fusion.7
  25.5 2.5 convolution_convert_fusion.3
  28.0 2.5 convolution_convert_fusion.2
  30.6 2.5 convolution_convert_fusion.4
  33.1 0.6 iota_compare_fusion.2
  33.9 0.1 fusion.13
  34.3 0.1 lt.76
  34.4 0.6 convert_compare_fusion
  35.0 0.1 lt.78
  35.2 0.1 lt.82
  35.3 0.3 reduce-window.9
  35.7 0.1 slice_reduce_fusion.6
  35.9 0.6 add_bitcast_fusion
  36.5 12.2 %psum.21 = f32[256]{0:T(256)S(1)} all-reduce(f32[256]{0:T(256)S(1)} %fusion.13), channel_id=1, replica_groups=mesh['kv'=8,'tp'=4] {'kv'}, use_global_device_ids=true, to_apply=%region_4.0 | all-reduce | flops 256 | bytes 2048 | tf_op jit(solution)/shard_map/psum | solution.py:93
  48.7 5.3 %copy.107 = f32[8,128,1024]{1,2,0:T(8,128)} copy(f32[8,128,1024]{2,1,0:T(8,128)} %param.19) | data formatting | bytes 8388608 | tf_op args[2]
  54.1 3.7 reduce-scatter.14.cloned.1.call-done
  57.8 37.1 %reduce-scatter.16.cloned.1.call-done = bf16[32,32]{1,0:T(8,128)(2,1)} async-done(((bf16[256,32]{1,0:T(8,128)(2,1)}), bf16[32,32]{1,0:T(8,128)(2,1)}) %reduce-scatter.16.cloned.1.call-update) | async-done | bytes 2064 | tf_op jit(solution)/shard_map/reduce_scatter | solution.py:105
  94.9 0.8 add_divide_fusion
  95.8 0.7 copy.117
  96.6 0.1 copy.111
  96.7 35.4 %reduce-scatter.18.cloned.1.call-done = bf16[32,1024]{1,0:T(8,128)(2,1)} async-done(((bf16[256,1024]{1,0:T(8,128)(2,1)}), bf16[32,1024]{1,0:T(8,128)(2,1)}) %reduce-scatter.18.cloned.1.call-update) | async-done | bytes 65552 | tf_op jit(solution)/shard_map/reduce_scatter | solution.py:102
  132.1 37.1 %reduce-scatter.20.cloned.1.call-done = bf16[32,1024]{1,0:T(8,128)(2,1)} async-done(((bf16[256,1024]{1,0:T(8,128)(2,1)}), bf16[32,1024]{1,0:T(8,128)(2,1)}) %reduce-scatter.20.cloned.1.call-update) | async-done | bytes 65552 | tf_op jit(solution)/shard_map/reduce_scatter | solution.py:99
  169.2 37.1 %reduce-scatter.12.cloned.1.call-done = bf16[32,1024]{1,0:T(8,128)(2,1)} async-done(((bf16[256,1024]{1,0:T(8,128)(2,1)}), bf16[32,1024]{1,0:T(8,128)(2,1)}) %reduce-scatter.12.cloned.1.call-update) | async-done | bytes 65552 | tf_op jit(solution)/shard_map/reduce_scatter | solution.py:96
  206.3 1.0 multiply_bitcast_fusion.2
  207.3 0.1 multiply_reduce_fusion.2
  207.6 0.1 multiply_reduce_fusion.1
  207.7 0.8 multiply_multiply_fusion.1
  208.6 0.1 broadcast_multiply_fusion.1
  208.7 1.9 fusion.7
  210.5 1.2 fusion.6
  211.8 1.1 slice_reduce_fusion.4
  212.9 0.1 multiply_subtract_fusion.1
  213.0 0.3 copy.120
  213.3 0.6 convolution_bitcast_fusion.5
  213.9 0.6 convolution_bitcast_fusion.4
  214.5 8.6 %fusion.2 = f32[8,4,8,128]{3,1,2,0:T(4,128)S(1)} fusion(f32[8,4,8,128]{3,1,2,0:T(4,128)S(1)} %convolution_bitcast_fusion.5, f32[8,4,8,128]{3,1,2,0:T(4,128)S(1)} %convolution_bitcast_fusion.4, f32[8,128,8,128]{1,3,2,0:T(8,128)} %bitcast.87), kind=kOutput, calls=%fused_computation.12 | convolution fusion | flops 50364416 | bytes 4587520 | tf_op jit(solution)/shard_map/nihd,ndhe->nihe/dot_general | solution.py:39
  223.2 0.7 convolution_bitcast_fusion.2
  223.9 6.7 %multiply_reduce_fusion = (f32[8,4,8]{1,2,0:T(8,128)S(1)}, f32[8,4,8,128]{3,1,2,0:T(4,128)S(1)}) fusion(f32[8,4,8,128]{3,1,2,0:T(4,128)S(1)} %convolution_bitcast_fusion.2, f32[8,128,8,128]{1,3,2,0:T(8,128)S(1)} %bitcast.89, f32[8,4,8,128]{3,2,1,0:T(8,128)S(1)} %get-tuple-element.22), kind=kOutput, calls=%fused_computation.46 | convolution fusion | flops 50429696 | bytes 4588544 | tf_op jit(solution)/shard_map/nihd,ndhe->nihe/dot_general | solution.py:41
  230.6 0.1 copy.128
  230.7 0.1 copy.129
  230.8 0.1 multiply_convert_fusion.2
  231.0 9.8 %all_gather.16 = bf16[256,1024]{1,0:T(8,128)(2,1)S(1)} all-gather(bf16[32,1024]{1,0:T(8,128)(2,1)S(1)} %bitcast.98), channel_id=1, replica_groups=mesh['kv'=8,'tp'=4] {'kv'}, dimensions={0}, use_global_device_ids=true | all-gather | bytes 589824 | tf_op jit(solution)/shard_map/all_gather | solution.py:144
  240.8 2.3 fusion.1
  243.1 1.7 copy.137
  244.9 19.6 %reduce-scatter.22.cloned.1.call-done = bf16[128,112]{1,0:T(8,128)(2,1)} async-done(((bf16[512,112]{1,0:T(8,128)(2,1)}), bf16[128,112]{1,0:T(8,128)(2,1)}) %reduce-scatter.22.cloned.1.call-update) | async-done | bytes 28688
  264.4 0.9 copy.138
  265.3 0.8 fusion.9
  266.1 12.2 %all_gather.17 = bf16[112,512]{1,0:T(8,128)(2,1)S(1)} all-gather(bf16[112,128]{1,0:T(8,128)(2,1)S(1)} %fusion.9), channel_id=1, replica_groups=mesh['kv'=8,'tp'=4] {'tp'}, dimensions={1}, use_global_device_ids=true | all-gather | bytes 143360 | tf_op jit(solution)/shard_map/all_gather | solution.py:154
  278.3 2.5 convolution_convert_fusion
  280.9 3.6 convolution_convert_fusion.1
  284.7 0.1 fusion.15
  284.8 12.6 %psum.23 = f32[112]{0:T(128)S(1)} all-reduce(f32[112]{0:T(128)S(1)} %fusion.15), channel_id=1, replica_groups=mesh['kv'=8,'tp'=4] {'kv'}, use_global_device_ids=true, to_apply=%region_16.17 | all-reduce | flops 112 | bytes 896 | tf_op jit(solution)/shard_map/psum | solution.py:159
  297.4 22.3 %all-gather.3.cloned.1.call-done = bf16[896,2752]{1,0:T(8,128)(2,1)} async-done(((bf16[112,2752]{1,0:T(8,128)(2,1)}), bf16[896,2752]{1,0:T(8,128)(2,1)}) %all-gather.3.cloned.1.call-update) | async-done | bytes 4931600 | tf_op jit(solution)/shard_map/all_gather | solution.py:162
  319.7 4.2 %reduce_sum.62 = bf16[112,2752]{1,0:T(8,128)(2,1)} reduce(bf16[8,112,2752]{2,1,0:T(8,128)(2,1)} %bitcast.91, bf16[]{:T(256)} %constant.56.clone.1), dimensions={0}, to_apply=%region_17.18 | reduce | flops 2157568 | bytes 5548034 | tf_op jit(solution)/shard_map/reduce_sum | solution.py:162
  323.8 54.2 %all-reduce.2.cloned.1.call-done = bf16[112,2752]{1,0:T(8,128)(2,1)} async-done(((bf16[112,2752]{1,0:T(8,128)(2,1)}), bf16[112,2752]{1,0:T(8,128)(2,1)}) %all-reduce.2.cloned.1.call-update) | async-done | bytes 616464 | tf_op jit(solution)/shard_map/psum | solution.py:161
  378.0 2.9 convolution_convert_fusion.6
  380.9 0.7 copy.139
  381.7 10.2 %bitcast_add_fusion = f32[8,128,8,128]{1,3,2,0:T(8,128)} fusion(f32[8,128,8,128]{1,3,2,0:T(8,128)} %bitcast.88, f32[8,4,8,128]{3,1,2,0:T(4,128)S(1)} %fusion.2, f32[8,8]{1,0:T(8,128)S(1)} %fusion.59, f32[8,4,8,128]{3,2,1,0:T(8,128)S(1)} %copy-done.2), kind=kOutput, calls=%fused_computation | convolution fusion | flops 52428800 | bytes 8651008 | tf_op jit(solution)/shard_map/nihd,nihe->ndhe/dot_general | solution.py:46
  391.9 5.4 %copy.133 = f32[8,128,1024]{2,1,0:T(8,128)} copy(f32[8,128,1024]{1,2,0:T(8,128)} %bitcast.90) | data formatting | bytes 8388608
  397.3 3.4 reduce-scatter.24.cloned.1.call-done
  400.7 0.9 copy.140
  401.6 0.9 fusion.8
  (84 shorter events, 1.7 us)
Async XLA Ops:
  7.2 271.2 %copy-start = (bf16[512,2752]{0,1:T(8,128)(2,1)S(1)}, bf16[512,2752]{0,1:T(8,128)(2,1)}, u32[]{:S(2)}) copy-start(bf16[512,2752]{0,1:T(8,128)(2,1)} %param.32) | copy-start | bytes 8454148
  7.2 20.8 %copy-start.6 = (f32[512]{0:T(512)S(1)}, f32[512]{0:T(512)}, u32[]{:S(2)}) copy-start(f32[512]{0:T(512)} %param.20) | copy-start | bytes 6148
  7.2 50.6 %reduce-scatter.14.cloned.1.call-start = ((), (), s32[]{:S(2)}) async-start(), calls=%async_computation.8 | async-start | bytes 73728 | tf_op jit(solution)/shard_map/reduce_scatter | solution.py:108
  23.7 71.2 %reduce-scatter.16.cloned.1.call-start = ((), (), s32[]{:S(2)}) async-start(), calls=%async_computation.9 | async-start | bytes 73728 | tf_op jit(solution)/shard_map/reduce_scatter | solution.py:105
  25.4 106.7 %reduce-scatter.18.cloned.1.call-start = ((), (), s32[]{:S(2)}) async-start(), calls=%async_computation.10 | async-start | bytes 589824 | tf_op jit(solution)/shard_map/reduce_scatter | solution.py:102
  27.9 5.8 %copy-start.11 = (s32[64]{0:T(128)S(1)}, s32[64]{0:T(128)}, u32[]{:S(2)}) copy-start(s32[64]{0:T(128)} %param.18) | copy-start | bytes 772
  27.9 6.2 %copy-start.14 = (f32[32]{0:T(128)S(1)}, f32[32]{0:T(128)}, u32[]{:S(2)}) copy-start(f32[32]{0:T(128)} %param.26) | copy-start | bytes 388
  27.9 6.3 %copy-start.15 = (f32[32]{0:T(128)S(1)}, f32[32]{0:T(128)}, u32[]{:S(2)}) copy-start(f32[32]{0:T(128)} %param.27) | copy-start | bytes 388
  28.0 141.2 %reduce-scatter.20.cloned.1.call-start = ((), (), s32[]{:S(2)}) async-start(), calls=%async_computation.11 | async-start | bytes 589824 | tf_op jit(solution)/shard_map/reduce_scatter | solution.py:99
  30.5 175.8 %reduce-scatter.12.cloned.1.call-start = ((), (), s32[]{:S(2)}) async-start(), calls=%async_computation.7 | async-start | bytes 589824 | tf_op jit(solution)/shard_map/reduce_scatter | solution.py:96
  33.1 231.3 %reduce-scatter.22.cloned.1.call-start = ((), (), s32[]{:S(2)}) async-start(), calls=%async_computation.14 | async-start | bytes 163840
  34.4 19.6 %copy-start.12 = (pred[256]{0:T(512)(128)(4,1)}, pred[256]{0:T(512)(128)(4,1)S(1)}, u32[]{:S(2)}) copy-start(pred[256]{0:T(512)(128)(4,1)S(1)} %lt.76) | copy-start | bytes 772
  206.3 2.4 copy-start.5
  213.3 9.8 %copy-start.3 = (f32[8,4,4,8]{1,2,3,0:T(4,128)S(1)}, f32[8,4,4,8]{1,2,3,0:T(4,128)}, u32[]{:S(2)}) copy-start(f32[8,4,4,8]{1,2,3,0:T(4,128)} %fusion.7) | copy-start | bytes 12292
  213.3 10.6 %copy-start.1 = (f32[8,128,1024]{1,2,0:T(8,128)S(1)}, f32[8,128,1024]{1,2,0:T(8,128)}, u32[]{:S(2)}) copy-start(f32[8,128,1024]{1,2,0:T(8,128)} %copy.107) | copy-start | bytes 12582916
  223.9 7.0 %copy-start.9 = (f32[128]{0:T(128)S(1)}, f32[128]{0:T(128)}, u32[]{:S(2)}) copy-start(f32[128]{0:T(128)} %param.28) | copy-start | bytes 1540
  230.6 34.7 %copy-start.4 = (bf16[64,4,128]{2,1,0:T(4,128)(2,1)S(1)}, bf16[64,4,128]{2,1,0:T(4,128)(2,1)}, u32[]{:S(2)}) copy-start(bf16[64,4,128]{2,1,0:T(4,128)(2,1)} %param.17) | copy-start | bytes 196612
  243.1 37.8 %copy-start.7 = (f32[512]{0:T(512)S(1)}, f32[512]{0:T(512)}, u32[]{:S(2)}) copy-start(f32[512]{0:T(512)} %param.30) | copy-start | bytes 6148
  244.8 74.9 %all-gather.3.cloned.1.call-start = ((), (), s32[]{:S(2)}) async-start(), calls=%async_computation.13 | async-start | bytes 5677056 | tf_op jit(solution)/shard_map/all_gather | solution.py:162
  280.9 97.1 %all-reduce.2.cloned.1.call-start = ((), (), s32[]{:S(2)}) async-start(), calls=%async_computation.12 | async-start | bytes 1261568 | tf_op jit(solution)/shard_map/psum | solution.py:161
  284.6 116.1 %reduce-scatter.24.cloned.1.call-start = ((), (), s32[]{:S(2)}) async-start(), calls=%async_computation.15 | async-start | bytes 163840
  323.8 57.8 %copy-start.2 = (f32[8,4,8,128]{3,2,1,0:T(8,128)S(1)}, f32[8,4,8,128]{3,2,1,0:T(8,128)}, u32[]{:S(2)}) copy-start(f32[8,4,8,128]{3,2,1,0:T(8,128)} %get-tuple-element.42) | copy-start | bytes 393220
  391.9 9.7 %copy-start.8 = (s32[256]{0:T(256)S(1)}, s32[256]{0:T(256)}, u32[]{:S(2)}) copy-start(s32[256]{0:T(256)} %add_bitcast_fusion) | copy-start | bytes 3076
  391.9 9.7 %copy-start.10 = (pred[256]{0:T(512)(128)(4,1)S(1)}, pred[256]{0:T(512)(128)(4,1)}, u32[]{:S(2)}) copy-start(pred[256]{0:T(512)(128)(4,1)} %convert_compare_fusion) | copy-start | bytes 772
  391.9 9.7 %copy-start.13 = (pred[256]{0:T(512)(128)(4,1)S(1)}, pred[256]{0:T(512)(128)(4,1)}, u32[]{:S(2)}) copy-start(pred[256]{0:T(512)(128)(4,1)} %copy-done.12) | copy-start | bytes 772
Sparse Core Ops, SparseCore 0:
  23.8 33.8 reduce-scatter.13
  61.3 33.4 reduce-scatter.15
  97.9 34.1 reduce-scatter.17
  135.0 34.1 reduce-scatter.19
  172.1 34.1 reduce-scatter.11
  244.9 19.4 reduce-scatter.21
  281.0 38.6 all-gather.2
  322.8 55.1 all-reduce.1
  381.8 18.9 reduce-scatter.23
